TPU v7x, 32 devices: a whole 2x2x4 slice. The times are simulated.
32 devices in a mesh: rep: 4 (over z), fs: 4 (over y, x), tp: 2 (over core).
Axes of the slice: x: 2, y: 2, z: 4, core: 2. Of those that a mesh axis runs over, the one named last changes fastest.
Arguments:
- tokens: bfloat16 [8192, 2048], P(('rep', 'fs')), may hold values from -6 to 6
- mix_gain: float32 [2048], replicated, may hold values from 0.1 to 1.9
- w_gate_b: bfloat16 [2048, 1024], P('fs', 'tp'), may hold values from -0.125 to 0.125
- w_gate_c: bfloat16 [2048, 1024], P('fs', 'tp'), may hold values from -0.125 to 0.125
- w_conv_in: bfloat16 [2048, 1024], P('fs', 'tp'), may hold values from -0.125 to 0.125
- conv_taps: float32 [3, 1024], P(None, 'tp'), may hold values from -3 to 3
- w_mix_out: bfloat16 [1024, 2048], P('tp', 'fs'), may hold values from -0.1875 to 0.1875
- ffn_gain: float32 [2048], replicated, may hold values from 0.1 to 1.9
- w_ffn_gate: bfloat16 [2048, 2816], P('fs', 'tp'), may hold values from -0.125 to 0.125
- w_ffn_up: bfloat16 [2048, 2816], P('fs', 'tp'), may hold values from -0.125 to 0.125
- w_ffn_down: bfloat16 [2816, 2048], P('tp', 'fs'), may hold values from -0.109375 to 0.109375
Outputs:
- layer_out: bfloat16 [8192, 2048], P(('rep', 'fs', 'tp'))
All inputs are finite; a program needn't handle non-finite values.
Results may differ from a plain program's by a relative error of at most 0.014.
Values may be sent and summed in bfloat16 or wider, within the bound.
A program may use at most 64 MiB of HBM per device.

v0:
```python
import jax
import jax.numpy as jnp
from jax import lax
from jax.sharding import PartitionSpec as P

LEN = 128


EPSILON = 1e-06


def rms_scale(values, gain):
    return values * lax.rsqrt(jnp.mean(values * values, axis=-1, keepdims=True) + EPSILON) * gain


def causal_mix(product_in, conv_taps):
    shaped = product_in.reshape(product_in.shape[0] // LEN, LEN, product_in.shape[1])
    padded = jnp.pad(shaped, ((0, 0), (2, 0), (0, 0)))
    convolved = (
        conv_taps[0] * padded[:, :-2]
        + conv_taps[1] * padded[:, 1:-1]
        + conv_taps[2] * padded[:, 2:]
    )
    return convolved.reshape(product_in.shape)


def local(
    tokens,
    mix_gain,
    w_gate_b,
    w_gate_c,
    w_conv_in,
    conv_taps,
    w_mix_out,
    ffn_gain,
    w_ffn_gate,
    w_ffn_up,
    w_ffn_down,
):
    normed = rms_scale(tokens.astype(jnp.float32), mix_gain).astype(jnp.bfloat16)
    shard_rows = (
        lax.all_gather(w_gate_b, "fs", axis=0, tiled=True),
        lax.all_gather(w_gate_c, "fs", axis=0, tiled=True),
        lax.all_gather(w_conv_in, "fs", axis=0, tiled=True),
    )
    gate_b, gate_c, conv_in = tuple(
        (jnp.dot(normed, weight, preferred_element_type=jnp.float32) for weight in shard_rows)
    )
    gated = (gate_b * causal_mix(gate_c * conv_in, conv_taps)).astype(jnp.bfloat16)
    mix_columns = lax.all_gather(w_mix_out, "fs", axis=1, tiled=True)
    row_count = normed.shape[0] // lax.axis_size("tp")
    branch = lax.psum_scatter(
        jnp.dot(gated, mix_columns, preferred_element_type=jnp.float32).astype(jnp.bfloat16),
        "tp",
        scatter_dimension=0,
        tiled=True,
    ).astype(jnp.float32)
    own_rows = lax.dynamic_slice_in_dim(tokens, lax.axis_index("tp") * row_count, row_count, 0)
    stream = own_rows.astype(jnp.float32) + branch
    normed_two = rms_scale(stream, ffn_gain).astype(jnp.bfloat16)
    gate_rows, up_rows = (
        lax.all_gather(w_ffn_gate, "fs", axis=0, tiled=True),
        lax.all_gather(w_ffn_up, "fs", axis=0, tiled=True),
    )
    shard_rows = lax.all_gather(normed_two, "tp", axis=0, tiled=True)
    gate_part = jnp.dot(shard_rows, gate_rows, preferred_element_type=jnp.float32)
    up_part = jnp.dot(shard_rows, up_rows, preferred_element_type=jnp.float32)
    hidden = (jax.nn.silu(gate_part) * up_part).astype(jnp.bfloat16)
    down_columns = lax.all_gather(w_ffn_down, "fs", axis=1, tiled=True)
    ffn_branch = lax.psum_scatter(
        jnp.dot(hidden, down_columns, preferred_element_type=jnp.float32).astype(jnp.bfloat16),
        "tp",
        scatter_dimension=0,
        tiled=True,
    ).astype(jnp.float32)
    return (stream + ffn_branch).astype(jnp.bfloat16)


def solution(mesh):
    in_specs = (
        P(("rep", "fs"), None),
        P(),
        P("fs", "tp"),
        P("fs", "tp"),
        P("fs", "tp"),
        P(None, "tp"),
        P("tp", "fs"),
        P(),
        P("fs", "tp"),
        P("fs", "tp"),
        P("tp", "fs"),
    )
    out_specs = P(("rep", "fs", "tp"), None)
    return jax.shard_map(local, mesh=mesh, in_specs=in_specs, out_specs=out_specs, check_vma=False)
```

profile of v0, /device:TPU:0, one launch (start us, length us, event | category | flops | bytes accessed | tf_op | source)
XLA Modules:
  0.0 424.1 jit_solution(1093069393383213584)
XLA Ops:
  6.5 0.7 all-gather.11.cloned.1.call-update
  7.3 0.7 all-gather.13.cloned.1.call-update
  8.1 0.7 all-gather.15.cloned.1.call-update
  9.9 37.2 %all-gather.11.cloned.1.call-done = bf16[2048,512]{1,0:T(8,128)(2,1)} async-done(((bf16[512,512]{1,0:T(8,128)(2,1)}), bf16[2048,512]{1,0:T(8,128)(2,1)}) %all-gather.11.cloned.1.call-update) | async-done | bytes 2097168 | tf_op jit(solution)/shard_map/all_gather | solution.py:43
  47.1 2.9 fusion.11
  50.0 34.2 %all-gather.13.cloned.1.call-done = bf16[2048,512]{1,0:T(8,128)(2,1)} async-done(((bf16[512,512]{1,0:T(8,128)(2,1)}), bf16[2048,512]{1,0:T(8,128)(2,1)}) %all-gather.13.cloned.1.call-update) | async-done | bytes 2097168 | tf_op jit(solution)/shard_map/all_gather | solution.py:44
  84.2 2.9 convolution_multiply_fusion.1
  87.4 33.7 %all-gather.15.cloned.1.call-done = bf16[512,2048]{1,0:T(8,128)(2,1)} async-done(((bf16[512,512]{1,0:T(8,128)(2,1)}), bf16[512,2048]{1,0:T(8,128)(2,1)}) %all-gather.15.cloned.1.call-update) | async-done | bytes 2097168 | tf_op jit(solution)/shard_map/all_gather | solution.py:50
  121.1 36.9 %all-gather.9.cloned.1.call-done = bf16[2048,512]{1,0:T(8,128)(2,1)} async-done(((bf16[512,512]{1,0:T(8,128)(2,1)}), bf16[2048,512]{1,0:T(8,128)(2,1)}) %all-gather.9.cloned.1.call-update) | async-done | bytes 2097168 | tf_op jit(solution)/shard_map/all_gather | solution.py:42
  158.0 5.9 %convolution_convert_fusion = bf16[512,2048]{1,0:T(8,128)(2,1)} fusion(bf16[512,2048]{1,0:T(8,128)(2,1)} %all-gather.15.cloned.1.call-done, f32[512,512]{1,0:T(8,128)S(1)} %bitcast.14, bf16[2048,512]{1,0:T(8,128)(2,1)} %all-gather.9.cloned.1.call-done, bf16[512,2048]{1,0:T(8,128)(2,1)S(1)} %copy-done, f32[2048]{0:T(1024)S(1)} %copy-done.4, ...), kind=kOutput, calls=%fused_computation.7 | convolution fusion | flops 2153250816 | bytes 9447424 | tf_op jit(solution)/shard_map/dot_general | solution.py:53
  164.0 0.5 all-gather.19.cloned.1.call-update
  164.6 9.3 %reduce-scatter.3.cloned.1.call-done = bf16[256,2048]{1,0:T(8,128)(2,1)} async-done(((bf16[512,2048]{1,0:T(8,128)(2,1)}), bf16[256,2048]{1,0:T(8,128)(2,1)}) %reduce-scatter.3.cloned.1.call-update) | async-done | bytes 1048592 | tf_op jit(solution)/shard_map/reduce_scatter | solution.py:52
  173.9 1.7 multiply_reduce_fusion
  175.6 1.5 multiply_convert_fusion
  177.2 0.7 all-gather.21.cloned.1.call-update
  177.9 0.7 all-gather.23.cloned.1.call-update
  178.8 63.7 %all-gather.19.cloned.1.call-done = bf16[2048,1408]{1,0:T(8,128)(2,1)} async-done(((bf16[512,1408]{1,0:T(8,128)(2,1)}), bf16[2048,1408]{1,0:T(8,128)(2,1)}) %all-gather.19.cloned.1.call-update) | async-done | bytes 5767184 | tf_op jit(solution)/shard_map/all_gather | solution.py:62
  242.5 12.1 %all-gather.17.cloned.1.call-done = bf16[512,2048]{1,0:T(8,128)(2,1)} async-done(((bf16[256,2048]{1,0:T(8,128)(2,1)}), bf16[512,2048]{1,0:T(8,128)(2,1)}) %all-gather.17.cloned.1.call-update) | async-done | bytes 2097168 | tf_op jit(solution)/shard_map/all_gather | solution.py:65
  254.7 8.2 %fusion.16 = f32[512,1408]{1,0:T(8,128)} fusion(bf16[512,2048]{1,0:T(8,128)(2,1)} %all-gather.17.cloned.1.call-done, bf16[2048,1408]{1,0:T(8,128)(2,1)} %all-gather.19.cloned.1.call-done), kind=kOutput, calls=%fused_computation.27 | convolution fusion | flops 2952790016 | bytes 10747904 | tf_op jit(solution)/shard_map/dot_general | solution.py:66
  262.9 60.5 %all-gather.21.cloned.1.call-done = bf16[2048,1408]{1,0:T(8,128)(2,1)} async-done(((bf16[512,1408]{1,0:T(8,128)(2,1)}), bf16[2048,1408]{1,0:T(8,128)(2,1)}) %all-gather.21.cloned.1.call-update) | async-done | bytes 5767184 | tf_op jit(solution)/shard_map/all_gather | solution.py:63
  323.4 67.4 %all-gather.23.cloned.1.call-done = bf16[1408,2048]{1,0:T(8,128)(2,1)} async-done(((bf16[1408,512]{1,0:T(8,128)(2,1)}), bf16[1408,2048]{1,0:T(8,128)(2,1)}) %all-gather.23.cloned.1.call-update) | async-done | bytes 5767184 | tf_op jit(solution)/shard_map/all_gather | solution.py:69
  390.8 13.8 %convolution_convert_fusion.1 = bf16[512,2048]{1,0:T(8,128)(2,1)} fusion(bf16[1408,2048]{1,0:T(8,128)(2,1)} %all-gather.23.cloned.1.call-done, bf16[512,2048]{1,0:T(8,128)(2,1)} %all-gather.17.cloned.1.call-done, bf16[2048,1408]{1,0:T(8,128)(2,1)} %all-gather.21.cloned.1.call-done, f32[512,1408]{1,0:T(8,128)} %fusion.16), kind=kOutput, calls=%fused_computation.8 | convolution fusion | flops 5910953984 | bytes 18612224 | tf_op jit(solution)/shard_map/dot_general | solution.py:71
  404.6 9.9 %reduce-scatter.5.cloned.1.call-done = bf16[256,2048]{1,0:T(8,128)(2,1)} async-done(((bf16[512,2048]{1,0:T(8,128)(2,1)}), bf16[256,2048]{1,0:T(8,128)(2,1)}) %reduce-scatter.5.cloned.1.call-update) | async-done | bytes 1048592 | tf_op jit(solution)/shard_map/reduce_scatter | solution.py:70
  414.5 2.7 add_convert_fusion
  (29 shorter events, 1.9 us)
Async XLA Ops:
  6.5 2.8 copy-start
  6.5 40.6 %all-gather.11.cloned.1.call-start = ((), (), s32[]{:S(2)}) async-start(), calls=%async_computation.3 | async-start | bytes 2621440 | tf_op jit(solution)/shard_map/all_gather | solution.py:43
  6.5 3.3 copy-start.3
  6.5 40.6 %copy-start.4 = (f32[2048]{0:T(1024)S(1)}, f32[2048]{0:T(1024)}, u32[]{:S(2)}) copy-start(f32[2048]{0:T(1024)} %param.12) | copy-start | bytes 24580
  7.3 76.9 %all-gather.13.cloned.1.call-start = ((), (), s32[]{:S(2)}) async-start(), calls=%async_computation.4 | async-start | bytes 2621440 | tf_op jit(solution)/shard_map/all_gather | solution.py:44
  8.0 113.1 %all-gather.15.cloned.1.call-start = ((), (), s32[]{:S(2)}) async-start(), calls=%async_computation.5 | async-start | bytes 2621440 | tf_op jit(solution)/shard_map/all_gather | solution.py:50
  8.7 149.2 %all-gather.9.cloned.1.call-start = ((), (), s32[]{:S(2)}) async-start(), calls=%async_computation.2 | async-start | bytes 2621440 | tf_op jit(solution)/shard_map/all_gather | solution.py:42
  9.3 164.5 %reduce-scatter.3.cloned.1.call-start = ((), (), s32[]{:S(2)}) async-start(), calls=%async_computation.6 | async-start | bytes 3145728 | tf_op jit(solution)/shard_map/reduce_scatter | solution.py:52
  163.9 11.7 %copy-start.2 = (f32[2048]{0:T(1024)S(1)}, f32[2048]{0:T(1024)}, u32[]{:S(2)}) copy-start(f32[2048]{0:T(1024)} %param.18) | copy-start | bytes 24580
  164.0 78.6 %all-gather.19.cloned.1.call-start = ((), (), s32[]{:S(2)}) async-start(), calls=%async_computation.8 | async-start | bytes 7208960 | tf_op jit(solution)/shard_map/all_gather | solution.py:62
  164.5 90.2 %all-gather.17.cloned.1.call-start = ((), (), s32[]{:S(2)}) async-start(), calls=%async_computation.7 | async-start | bytes 3145728 | tf_op jit(solution)/shard_map/all_gather | solution.py:65
  173.9 1.8 copy-start.1
  177.1 146.3 %all-gather.21.cloned.1.call-start = ((), (), s32[]{:S(2)}) async-start(), calls=%async_computation.9 | async-start | bytes 7208960 | tf_op jit(solution)/shard_map/all_gather | solution.py:63
  177.9 212.9 %all-gather.23.cloned.1.call-start = ((), (), s32[]{:S(2)}) async-start(), calls=%async_computation.10 | async-start | bytes 7208960 | tf_op jit(solution)/shard_map/all_gather | solution.py:69
  178.6 235.9 %reduce-scatter.5.cloned.1.call-start = ((), (), s32[]{:S(2)}) async-start(), calls=%async_computation.11 | async-start | bytes 3145728 | tf_op jit(solution)/shard_map/reduce_scatter | solution.py:70
Sparse Core Ops, SparseCore 0:
  9.2 37.8 all-gather.10
  49.0 35.1 all-gather.12
  86.0 35.0 all-gather.14
  122.8 35.1 all-gather.8
  164.1 9.7 reduce-scatter.2
  175.6 66.9 all-gather.18
  244.1 10.5 all-gather.16
  256.5 66.8 all-gather.20
  325.2 65.5 all-gather.22
  404.8 9.7 reduce-scatter.4
where the time goes:
time: 424 us
  waiting for transfers between devices  369 us (87%)
  matrix products  33.8 us (8%)
  between operations  13.6 us (3%)
  other arithmetic  6.75 us (2%)
    all_gather x1, waiting for transfers between devices, local(): down_columns = lax.all_gather(w_ffn_down, 'fs', axis=1, tiled=True)  67.4 us
    all_gather x1, waiting for transfers between devices, local(): lax.all_gather(w_ffn_gate, 'fs', axis=0, tiled=True)  63.7 us
    all_gather x1, waiting for transfers between devices, local(): lax.all_gather(w_ffn_up, 'fs', axis=0, tiled=True)  60.5 us
    all_gather x1, waiting for transfers between devices, local(): lax.all_gather(w_gate_c, 'fs', axis=0, tiled=True)  37.2 us
    all_gather x1, waiting for transfers between devices, local(): lax.all_gather(w_gate_b, 'fs', axis=0, tiled=True)  36.9 us
    all_gather x1, waiting for transfers between devices, local(): lax.all_gather(w_conv_in, 'fs', axis=0, tiled=True)  34.2 us
    all_gather x1, waiting for transfers between devices, local(): mix_columns = lax.all_gather(w_mix_out, 'fs', axis=1, tiled=True)  33.7 us
    dot_general x1, matrix products, local(): jnp.dot(hidden, down_columns, preferred_element_type=jnp.float32)  13.8 us
  transfers between devices with their start and end apart: 10, of which 10 were waited for; matrix products, arithmetic and copies ran while one was open for 4% of the time, Pallas kernels for 0%

commit v1 on v0

v1 whole, which is shorter than its diff:
```python
import functools

import jax
import jax.numpy as jnp
from jax import lax
from jax.experimental import pallas as pl
from jax.experimental.pallas import tpu as pltpu
from jax.sharding import PartitionSpec as P

LEN = 128
LANES = 128
EPSILON = 1e-06
MESH = pl.DeviceIdType.MESH
F32 = jnp.float32
BF16 = jnp.bfloat16


def rms_scale(values, gain):
    return values * lax.rsqrt(jnp.mean(values * values, axis=-1, keepdims=True) + EPSILON) * gain


def layer_kernel(
    tokens, wb, wc, wi, wm_in, wgu_in, wd_in, mix_gain, taps, ffn_gain,
    out,
    tok, normed, n2, WA, WM, WG, WD, gated, MP, RS, CB, RZ, hidden, OS, OW, RO, ZC, RF,
    load_sem, ds, dr, fs_, fr, tz, ts, sib_s, sib_r, z_s, z_r, n_s, n_r, o_s, o_r, q_s, q_r,
):
    n_fs, rows_d, _ = WA.shape
    ch = gated.shape[1]
    hid = hidden.shape[1]
    chip_rows = tokens.shape[0]
    blk = chip_rows // 2
    width = tokens.shape[1]
    cols = WM.shape[2]

    r = lax.axis_index("rep")
    f = lax.axis_index("fs")
    t = lax.axis_index("tp")
    p = lax.rem(r, 2)
    z_dev = {"rep": r + 1 - 2 * p}
    x_of = f + 1 - 2 * lax.rem(f, 2)
    y_of = lax.rem(f + 2, 4)
    d_of = lax.rem(x_of + 2, 4)
    x_dev, y_dev, s_dev = {"fs": x_of}, {"fs": y_of}, {"tp": 1 - t}

    def row_block(j, core):
        return pl.ds(pl.multiple_of(j * chip_rows + core * blk, blk), blk)

    chan = pl.ds(pl.multiple_of(p * ch, ch), ch)
    loads = []

    def load(src, dst):
        c = pltpu.make_async_copy(src, dst, load_sem.at[len(loads)])
        c.start()
        loads.append(c)
        return c

    l_wa = [load(w.at[:, chan], WA.at[f, :, pl.ds(i * ch, ch)]) for i, w in enumerate((wb, wc, wi))]
    l_tok = load(tokens, tok.at[pl.ds(pl.multiple_of(p * chip_rows, chip_rows), chip_rows)])
    l_wm = load(wm_in.at[chan, :], WM.at[f])
    l_wg = load(wgu_in, WG.at[f])
    l_wd = load(wd_in.at[pl.ds(pl.multiple_of(p * hid, 16), hid), :], WD.at[f])

    barrier = pltpu.get_barrier_semaphore()
    for dev in (x_dev, y_dev, z_dev, s_dev):
        pl.semaphore_signal(barrier, inc=1, device_id=dev, device_id_type=MESH)
    pl.semaphore_wait(barrier, 4)

    def remote(src, dst, s, rcv, dev):
        return pltpu.make_async_remote_copy(
            src_ref=src, dst_ref=dst, send_sem=s, recv_sem=rcv, device_id=dev, device_id_type=MESH
        )

    pieces = []
    for buf, parts in ((WA, 2), (WM, 1), (WG, 4), (WD, 2)):
        n = buf.shape[1] // parts
        pieces += [(buf, i * n, n) for i in range(parts)]

    def direct(k):
        buf, r0, n = pieces[k]
        ref = buf.at[f, pl.ds(r0, n)]
        return [remote(ref, ref, ds.at[k, c], dr.at[k, c], dev) for c, dev in ((0, x_dev), (1, y_dev))]

    def forward(k):
        buf, r0, n = pieces[k]
        a = buf.at[x_of, pl.ds(r0, n // 2)]
        b = buf.at[y_of, pl.ds(r0 + n // 2, n // 2)]
        return [
            remote(b, b, fs_.at[k, 0], fr.at[k, 0], x_dev),
            remote(a, a, fs_.at[k, 1], fr.at[k, 1], y_dev),
        ]

    sent = []

    def start(copies):
        for c in copies:
            c.start()
            sent.append(c)
        return copies

    D, F = {}, {}

    def send(k):
        D[k] = start(direct(k))

    def step(k, *more):
        for c in D[k]:
            c.wait_recv()
        F[k] = start(forward(k))
        for m in more:
            send(m)

    def arrived(*ks):
        for k in ks:
            for c in F[k]:
                c.wait_recv()

    for c in l_wa:
        c.wait()
    send(0)
    send(1)
    l_tok.wait()
    own = tok.at[row_block(p, t)]
    tz_copy = start([remote(own, own, tz.at[0], tz.at[1], z_dev)])[0]

    def norm_rows(base):
        def body(i, _):
            rows = pl.ds(pl.multiple_of(base + i * 64, 64), 64)
            normed[rows, :] = rms_scale(tok[rows, :].astype(F32), mix_gain[...]).astype(BF16)
            return 0

        lax.fori_loop(0, chip_rows // 64, body, 0)

    norm_rows(p * chip_rows)
    l_wm.wait()
    l_wg.wait()
    l_wd.wait()
    step(0, 2)
    step(1)
    tz_copy.wait_recv()
    got = tok.at[row_block(1 - p, t)]
    ts_copy = start([remote(got, got, ts.at[0], ts.at[1], s_dev)])[0]
    step(2, 3, 4)
    ts_copy.wait_recv()
    norm_rows((1 - p) * chip_rows)
    arrived(0, 1)

    tap = [taps[pl.ds(i, 1), chan] for i in range(3)]
    pos = lax.rem(lax.broadcasted_iota(jnp.int32, (blk, ch), 0), LEN)

    def mix_body(i, _):
        rows = pl.ds(pl.multiple_of(i * blk, blk), blk)
        x = normed[rows, :]

        def proj(q):
            w = WA[:, :, q * ch:(q + 1) * ch].reshape(width, ch)
            return jnp.dot(x, w, preferred_element_type=F32)

        pr = proj(1) * proj(2)
        one = jnp.where(pos >= 1, pltpu.roll(pr, 1, 0), 0.0)
        two = jnp.where(pos >= 2, pltpu.roll(pr, 2, 0), 0.0)
        conv = tap[0] * two + tap[1] * one + tap[2] * pr
        gated[rows, :] = (proj(0) * conv).astype(BF16)
        return 0

    lax.fori_loop(0, 2 * chip_rows // blk, mix_body, 0)
    arrived(2)

    def mix_out(j, core):
        rows = row_block(j, core)
        g = gated[rows, :]
        for s in range(n_fs):
            MP[rows, s * cols:(s + 1) * cols] = jnp.dot(
                g, WM[s], preferred_element_type=F32
            ).astype(BF16)

    sib = []
    for j in range(2):
        mix_out(j, 1 - t)
        sib += start([remote(MP.at[row_block(j, 1 - t)], RS.at[j], sib_s.at[j], sib_r.at[j], s_dev)])
    zc = []
    for j in range(2):
        mix_out(j, t)
        sib[j].wait_recv()

        def add_body(i, _, j=j):
            rows = pl.ds(pl.multiple_of(i * 64, 64), 64)
            mine = pl.ds(pl.multiple_of(j * chip_rows + t * blk + i * 64, 64), 64)
            CB[j, rows, :] = (MP[mine, :].astype(F32) + RS[j, rows, :].astype(F32)).astype(BF16)
            return 0

        lax.fori_loop(0, blk // 64, add_body, 0)
        zc += start([remote(CB.at[j], RZ.at[j], z_s.at[j], z_r.at[j], z_dev)])

    step(3, 5)
    step(4, 6)
    step(5, 7)
    nb = []

    def stream_block(j):
        zc[j].wait_recv()

        def body(i, _):
            rows = pl.ds(pl.multiple_of(i * 64, 64), 64)
            mine = pl.ds(pl.multiple_of(j * chip_rows + t * blk + i * 64, 64), 64)
            stream = tok[mine, :].astype(F32) + (CB[j, rows, :].astype(F32) + RZ[j, rows, :].astype(F32))
            n2[mine, :] = rms_scale(stream, ffn_gain[...]).astype(BF16)
            return 0

        lax.fori_loop(0, blk // 64, body, 0)
        ref = n2.at[row_block(j, t)]
        nb.extend(start([remote(ref, ref, n_s.at[j], n_r.at[j], s_dev)]))

    stream_block(0)
    step(6, 8)
    step(7)
    stream_block(1)
    arrived(3, 4, 5, 6)
    nb[0].wait_recv()

    def ffn_rows(j):
        def body(i, _):
            rows = pl.ds(pl.multiple_of(j * chip_rows + i * blk, blk), blk)
            x = n2[rows, :]
            full = hid // LANES
            for c in range(full):
                w = WG[:, :, 2 * c * LANES:2 * (c + 1) * LANES].reshape(width, 2 * LANES)
                zz = jnp.dot(x, w, preferred_element_type=F32)
                g, u = zz[:, :LANES], zz[:, LANES:]
                hidden[rows, c * LANES:(c + 1) * LANES] = (g / (1.0 + jnp.exp(-g)) * u).astype(BF16)
            rest = hid - full * LANES
            if rest:
                w = WG[:, :, 2 * full * LANES:].reshape(width, 2 * rest)
                zz = jnp.dot(x, w, preferred_element_type=F32)
                g, u = zz[:, :rest], zz[:, rest:]
                hidden[rows, full * LANES:] = (g / (1.0 + jnp.exp(-g)) * u).astype(BF16)
            return 0

        lax.fori_loop(0, chip_rows // blk, body, 0)

    ffn_rows(0)
    nb[1].wait_recv()
    ffn_rows(1)
    step(8)

    so, qo = [], []

    def down_send(k, s):
        for j in range(2):
            h = hidden[row_block(j, 1 - t), :]
            OS[s, j] = jnp.dot(h, WD[s], preferred_element_type=F32).astype(BF16)
        so.extend(start([remote(OS.at[s], RO.at[s], o_s.at[k], o_r.at[k], s_dev)]))
        for j in range(2):
            h = hidden[row_block(j, t), :]
            OW[s, j] = jnp.dot(h, WD[s], preferred_element_type=F32).astype(BF16)

    def down_pair(k, s):
        so[k].wait_recv()
        ZC[s] = (OW[s, 1 - p].astype(F32) + RO[s, 1 - p].astype(F32)).astype(BF16)
        qo.extend(start([remote(ZC.at[s], RF.at[s], q_s.at[k], q_r.at[k], z_dev)]))

    def finish(k, s):
        qo[k].wait_recv()
        cs = pl.ds(pl.multiple_of(s * cols, cols), cols)
        mine = row_block(p, t)
        stream = tok[mine, cs].astype(F32) + (CB[p, :, cs].astype(F32) + RZ[p, :, cs].astype(F32))
        branch = OW[s, p].astype(F32) + RO[s, p].astype(F32) + RF[s].astype(F32)
        out[:, cs] = (stream + branch).astype(BF16)

    slots = (f, x_of, y_of, d_of)
    down_send(0, slots[0])
    down_send(1, slots[1])
    down_pair(0, slots[0])
    down_send(2, slots[2])
    down_pair(1, slots[1])
    down_pair(2, slots[2])
    arrived(7, 8)
    down_send(3, slots[3])
    down_pair(3, slots[3])
    for k in range(4):
        finish(k, slots[k])
    for c in sent:
        c.wait_send()


def paired_local(
    tokens, mix_gain, w_gate_b, w_gate_c, w_conv_in, conv_taps, w_mix_out, ffn_gain,
    w_ffn_gate, w_ffn_up, w_ffn_down,
):
    chip_rows, width = tokens.shape
    n_fs = lax.axis_size("fs")
    rows_d = w_gate_b.shape[0]
    ch = w_gate_b.shape[1] // 2
    hid = w_ffn_gate.shape[1] // 2
    cols = w_mix_out.shape[1]
    blk = chip_rows // 2
    p = lax.rem(lax.axis_index("rep"), 2)
    half = [lax.dynamic_slice_in_dim(w, p * hid, hid, 1) for w in (w_ffn_gate, w_ffn_up)]
    parts = []
    for c in range(0, hid, LANES):
        parts += [h[:, c:c + LANES] for h in half]
    wgu = jnp.concatenate(parts, axis=1)

    VM = functools.partial(pltpu.VMEM, dtype=BF16)
    dma = lambda *s: pltpu.SemaphoreType.DMA(s)
    n_pieces = 9
    any_, vmem = pl.BlockSpec(memory_space=pl.ANY), pl.BlockSpec(memory_space=pltpu.VMEM)
    return pl.pallas_call(
        layer_kernel,
        out_shape=jax.ShapeDtypeStruct((blk, width), BF16),
        in_specs=[any_] * 7 + [vmem] * 3,
        out_specs=vmem,
        scratch_shapes=[
            pltpu.VMEM((2 * chip_rows, width), BF16),
            pltpu.VMEM((2 * chip_rows, width), BF16),
            pltpu.VMEM((2 * chip_rows, width), BF16),
            pltpu.VMEM((n_fs, rows_d, 3 * ch), BF16),
            pltpu.VMEM((n_fs, ch, cols), BF16),
            pltpu.VMEM((n_fs, rows_d, 2 * hid), BF16),
            pltpu.VMEM((n_fs, hid, cols), BF16),
            pltpu.VMEM((2 * chip_rows, ch), BF16),
            pltpu.VMEM((2 * chip_rows, width), BF16),
            pltpu.VMEM((2, blk, width), BF16),
            pltpu.VMEM((2, blk, width), BF16),
            pltpu.VMEM((2, blk, width), BF16),
            pltpu.VMEM((2 * chip_rows, hid), BF16),
            pltpu.VMEM((n_fs, 2, blk, cols), BF16),
            pltpu.VMEM((n_fs, 2, blk, cols), BF16),
            pltpu.VMEM((n_fs, 2, blk, cols), BF16),
            pltpu.VMEM((n_fs, blk, cols), BF16),
            pltpu.VMEM((n_fs, blk, cols), BF16),
            dma(7),
            dma(n_pieces, 2), dma(n_pieces, 2), dma(n_pieces, 2), dma(n_pieces, 2),
            dma(2), dma(2),
            dma(2), dma(2), dma(2), dma(2), dma(2), dma(2),
            dma(4), dma(4), dma(4), dma(4),
        ],
        compiler_params=pltpu.CompilerParams(
            collective_id=0, has_side_effects=True, vmem_limit_bytes=60 * 2**20
        ),
    )(
        tokens, w_gate_b, w_gate_c, w_conv_in, w_mix_out, wgu, w_ffn_down,
        mix_gain.reshape(1, width), conv_taps, ffn_gain.reshape(1, width),
    )


def causal_mix(product_in, conv_taps):
    shaped = product_in.reshape(product_in.shape[0] // LEN, LEN, product_in.shape[1])
    padded = jnp.pad(shaped, ((0, 0), (2, 0), (0, 0)))
    convolved = (
        conv_taps[0] * padded[:, :-2]
        + conv_taps[1] * padded[:, 1:-1]
        + conv_taps[2] * padded[:, 2:]
    )
    return convolved.reshape(product_in.shape)


def general_local(
    tokens, mix_gain, w_gate_b, w_gate_c, w_conv_in, conv_taps, w_mix_out, ffn_gain,
    w_ffn_gate, w_ffn_up, w_ffn_down,
):
    def scatter(product):
        return lax.psum_scatter(
            product.astype(BF16), "tp", scatter_dimension=0, tiled=True
        ).astype(F32)

    def dot(a, b):
        return jnp.dot(a, b, preferred_element_type=F32)

    def rows(w):
        return lax.all_gather(w, "fs", axis=0, tiled=True)

    normed = rms_scale(tokens.astype(F32), mix_gain).astype(BF16)
    gate_b, gate_c, conv_in = (dot(normed, rows(w)) for w in (w_gate_b, w_gate_c, w_conv_in))
    gated = (gate_b * causal_mix(gate_c * conv_in, conv_taps)).astype(BF16)
    row_count = normed.shape[0] // lax.axis_size("tp")
    branch = scatter(dot(gated, lax.all_gather(w_mix_out, "fs", axis=1, tiled=True)))
    own = lax.dynamic_slice_in_dim(tokens, lax.axis_index("tp") * row_count, row_count, 0)
    stream = own.astype(F32) + branch
    normed_two = lax.all_gather(
        rms_scale(stream, ffn_gain).astype(BF16), "tp", axis=0, tiled=True
    )
    hidden = (jax.nn.silu(dot(normed_two, rows(w_ffn_gate))) * dot(normed_two, rows(w_ffn_up))).astype(BF16)
    ffn_branch = scatter(dot(hidden, lax.all_gather(w_ffn_down, "fs", axis=1, tiled=True)))
    return (stream + ffn_branch).astype(BF16)


def solution(mesh):
    in_specs = (
        P(("rep", "fs"), None),
        P(),
        P("fs", "tp"),
        P("fs", "tp"),
        P("fs", "tp"),
        P(None, "tp"),
        P("tp", "fs"),
        P(),
        P("fs", "tp"),
        P("fs", "tp"),
        P("tp", "fs"),
    )
    out_specs = P(("rep", "fs", "tp"), None)
    size = mesh.shape
    paired = size["tp"] == 2 and size["fs"] == 4 and size["rep"] % 2 == 0
    body = paired_local if paired else general_local
    return jax.shard_map(body, mesh=mesh, in_specs=in_specs, out_specs=out_specs, check_vma=False)
```

time: 424 us -> 141 us (0.33)
  waiting for transfers between devices: 369 us -> 0 us
  Pallas kernels: 0 us -> 132 us
  matrix products: 33.8 us -> 0 us
  between operations: 13.6 us -> 0.03 us
  local copies, waits for them, and re-layouts: 0.03 us -> 8.9 us
  other arithmetic: 6.75 us -> 0 us
    all_gather x8 -> x0, waiting for transfers between devices: 346 us -> none  [the longest x1 67.4 us: local(): down_columns = lax.all_gather(w_ffn_down, 'fs', axis=1, tiled=True)]
    pallas_call x0 -> x1, Pallas kernels: none -> 132 us  [paired_local(): pl.pallas_call(layer_kernel, out_shape=jax.ShapeDtypeStruct((blk, width),...]
    dot_general x5 -> x0, matrix products: 33.8 us -> none  [the longest x1 13.8 us: local(): jnp.dot(hidden, down_columns, preferred_element_type=jnp.float32)]
    reduce_scatter x2 -> x0, waiting for transfers between devices: 19.2 us -> none  [the longest x1 9.89 us: local(): lax.psum_scatter(jnp.dot(hidden, down_columns, preferred_element_type=jnp...]
    unnamed x10 -> x0, waiting for transfers between devices: 4.55 us -> none
  transfers between devices with their start and end apart: 10 -> 0, of which waited for: 10 -> 0; matrix products, arithmetic and copies ran while one was open for 4% -> 0% of each run, Pallas kernels for 0% -> 0%
where the time goes in v1:
time: 141 us
  Pallas kernels  132 us (94%)
  local copies, waits for them, and re-layouts  8.9 us (6%)
    pallas_call x1, Pallas kernels, paired_local(): pl.pallas_call(layer_kernel, out_shape=jax.ShapeDtypeStruct((blk, width),...  132 us
    slice x2, local copies, waits for them, and re-layouts, paired_local(): parts += [h[:, c:c + LANES] for h in half]  3.31 us
    concatenate x1, local copies, waits for them, and re-layouts, paired_local(): wgu = jnp.concatenate(parts, axis=1)  3.29 us

profile of v1, /device:TPU:0, one launch (start us, length us, event | category | flops | bytes accessed | tf_op | source)
XLA Modules:
  0.0 140.9 jit_solution(9712892160953286993)
XLA Ops:
  0.0 1.1 constant_dynamic-slice_fusion.10
  1.1 2.2 %constant_dynamic-slice_fusion = (bf16[512,128]{1,0:T(8,128)(2,1)S(1)}, bf16[512,128]{1,0:T(8,128)(2,1)S(1)}, bf16[512,128]{1,0:T(8,128)(2,1)S(1)}, bf16[512,128...) fusion(bf16[512,1408]{1,0:T(8,128)(2,1)} %param.20, ...), kind=kLoop, calls=%fused_computation | loop fusion | bytes 2621460 | tf_op jit(solution)/shard_map/slice | solution.py:301
  3.3 3.3 %concatenate.3.wgu_in = bf16[512,1408]{1,0:T(8,128)(2,1)} concatenate(bf16[512,128]{1,0:T(8,128)(2,1)S(1)} %get-tuple-element.15, bf16[512,128]{1,0:T(8,128)(2,1)S(1)} %get-tuple-element.9, bf16[512,128]{1,0:T(8,128)(2,1)S(1)} %get-tuple-element.16, bf16[512,128]{1,0:T(8,128)(2,1)S(1)} %get-tuple-element.8, bf16[512,128]{1,0:T(8,128)(2,1)S(1)} %get-tuple-element.17, ...), dimensions={1} | concatenate | bytes 2883584 | tf_op jit(solution)/shard_map/concatenate | solution.py:302
  6.6 132.0 %shard_map.109 = bf16[256,2048]{1,0:T(8,128)(2,1)} custom-call(bf16[512,2048]{1,0:T(8,128)(2,1)} %tokens.1, bf16[512,512]{1,0:T(8,128)(2,1)} %wb.1, bf16[512,512]{1,0:T(8,128)(2,1)} %wc.1, bf16[512,512]{1,0:T(8,128)(2,1)} %wi.1, bf16[512,512]{1,0:T(8,128)(2,1)} %wm_in.1, bf16[512,1408]{1,0:T(8,128)(2,1)} %concatenate.3.wgu_in, bf16[1408,512]{1,0:T(8,128)(2,1)} %wd_in.1, ...), custom_call_target="tpu_custom_call" | custom-call | tf_op jit(solution)/shard_map/pallas_call | solution.py:308
  138.6 2.3 %copy.13 = bf16[256,2048]{1,0:T(8,128)(2,1)} copy(bf16[256,2048]{1,0:T(8,128)(2,1)} %shard_map.109) | data formatting | bytes 2097152

commit v2 on v1

v2 whole, which is shorter than its diff:
```python
import jax
import jax.numpy as jnp
from jax import lax
from jax.experimental import pallas as pl
from jax.experimental.pallas import tpu as pltpu
from jax.sharding import PartitionSpec as P

LEN = 128
LANES = 128
EPSILON = 1e-06
MESH = pl.DeviceIdType.MESH
F32 = jnp.float32
BF16 = jnp.bfloat16


def rms_scale(values, gain):
    return values * lax.rsqrt(jnp.mean(values * values, axis=-1, keepdims=True) + EPSILON) * gain


N_CHUNKS = 4
PIECES = (2, 1, 4, 2)


def layer_kernel(
    tokens, wb, wc, wi, wm_in, wg_in, wu_in, wd_in, mix_gain, taps, ffn_gain,
    out,
    tok, normed, n2, WA, WM, WG, WD, tile, gated, MP, RS, CB, RZ, hidden, OP, RO, ZC, RF,
    load_sem, ds, dr, fs_, fr, tz_s, tz_r, ts_s, ts_r, sib_s, sib_r, z_s, z_r, n_s, n_r,
    o_s, o_r, q_s, q_r,
):
    n_fs, rows_d, _ = WA.shape
    ch = gated.shape[1]
    hid = hidden.shape[1]
    width = tokens.shape[1]
    half = tokens.shape[0] // 4
    cols = WM.shape[2]
    full, rest = hid // LANES, hid % LANES

    r = lax.axis_index("rep")
    f = lax.axis_index("fs")
    t = lax.axis_index("tp")
    p = lax.rem(r, 2)
    z_dev = {"rep": r + 1 - 2 * p}
    x_of = f + 1 - 2 * lax.rem(f, 2)
    y_of = lax.rem(f + 2, 4)
    d_of = lax.rem(x_of + 2, 4)
    x_dev, y_dev, s_dev = {"fs": x_of}, {"fs": y_of}, {"tp": 1 - t}

    def part(c, core):
        return pl.ds(pl.multiple_of((2 * c + core) * half, half), half)

    def chunk(c):
        return pl.ds(pl.multiple_of(2 * c * half, 2 * half), 2 * half)

    chan = pl.ds(pl.multiple_of(p * ch, ch), ch)
    loads = []

    def load(src, dst):
        c = pltpu.make_async_copy(src, dst, load_sem.at[len(loads)])
        c.start()
        loads.append(c)
        return c

    l_wa = [load(w.at[:, chan], WA.at[f, :, pl.ds(i * ch, ch)]) for i, w in enumerate((wb, wc, wi))]
    l_tok = [
        load(tokens.at[pl.ds((2 * core + h) * half, half)], tok.at[part(2 * h + p, core)])
        for h in range(2) for core in range(2)
    ]
    l_rest = [load(wm_in.at[chan, :], WM.at[f])]
    far = (full + (1 if rest else 0)) * LANES
    for i, w in enumerate((wg_in, wu_in)):
        for c in range(full):
            col = pl.ds(pl.multiple_of(p * far + c * LANES, LANES), LANES)
            l_rest.append(load(w.at[:, col], WG.at[f, :, pl.ds((2 * c + i) * LANES, LANES)]))
        if rest:
            l_rest.append(load(w.at[:, pl.ds(full * LANES, LANES)], tile.at[i]))
    aligned = full * LANES
    l_rest.append(load(wd_in.at[pl.ds(pl.multiple_of(p * far, LANES), aligned)], WD.at[f, pl.ds(0, aligned)]))
    if rest:
        l_rest.append(load(
            wd_in.at[pl.ds(pl.multiple_of(aligned + p * rest, rest), rest)],
            WD.at[f, pl.ds(aligned, rest)],
        ))

    barrier = pltpu.get_barrier_semaphore()
    for dev in (x_dev, y_dev, z_dev, s_dev):
        pl.semaphore_signal(barrier, inc=1, device_id=dev, device_id_type=MESH)
    pl.semaphore_wait(barrier, 4)

    def remote(src, dst, s, rcv, dev):
        return pltpu.make_async_remote_copy(
            src_ref=src, dst_ref=dst, send_sem=s, recv_sem=rcv, device_id=dev, device_id_type=MESH
        )

    pieces = []
    for buf, parts in zip((WA, WM, WG, WD), PIECES):
        n = buf.shape[1] // parts
        pieces += [(buf, i * n, n) for i in range(parts)]

    def direct(k):
        buf, r0, n = pieces[k]
        ref = buf.at[f, pl.ds(r0, n)]
        return [remote(ref, ref, ds.at[k, c], dr.at[k, c], dev) for c, dev in ((0, x_dev), (1, y_dev))]

    def forward(k):
        buf, r0, n = pieces[k]
        a = buf.at[x_of, pl.ds(r0, n // 2)]
        b = buf.at[y_of, pl.ds(r0 + n // 2, n // 2)]
        return [
            remote(b, b, fs_.at[k, 0], fr.at[k, 0], x_dev),
            remote(a, a, fs_.at[k, 1], fr.at[k, 1], y_dev),
        ]

    sent = []

    def start(*copies):
        for c in copies:
            c.start()
            sent.append(c)
        return copies

    D, F = {}, {}

    def send(*ks):
        for k in ks:
            D[k] = start(*direct(k))

    def step(k, *more):
        for c in D[k]:
            c.wait_recv()
        F[k] = start(*forward(k))
        send(*more)

    def arrived(*ks):
        for k in ks:
            for c in F[k]:
                c.wait_recv()

    for c in l_wa:
        c.wait()
    send(0, 1)
    for c in l_tok:
        c.wait()
    tz, ts = [], []
    for h in range(2):
        ref = tok.at[part(2 * h + p, t)]
        tz += start(remote(ref, ref, tz_s.at[h], tz_r.at[h], z_dev))

    def relay(h):
        tz[h].wait_recv()
        ref = tok.at[part(2 * h + 1 - p, t)]
        ts.extend(start(remote(ref, ref, ts_s.at[h], ts_r.at[h], s_dev)))

    def norm_chunk(c):
        def body(i, _):
            rows = pl.ds(pl.multiple_of(2 * c * half + i * 64, 64), 64)
            normed[rows, :] = rms_scale(tok[rows, :].astype(F32), mix_gain[...]).astype(BF16)
            return 0

        lax.fori_loop(0, 2 * half // 64, body, 0)

    norm_chunk(p)
    norm_chunk(2 + p)
    for c in l_rest:
        c.wait()
    if rest:
        gate, up = tile[0].astype(F32), tile[1].astype(F32)
        lane = lax.broadcasted_iota(jnp.int32, gate.shape, 1)
        low = jnp.where(lane < rest, gate, pltpu.roll(up, rest, 1))
        high = jnp.where(lane < rest, pltpu.roll(gate, rest, 1), up)
        WG[f, :, 2 * aligned:] = jnp.where(p == 0, low, high).astype(BF16)
    step(0, 2)
    relay(0)
    step(1)
    ts[0].wait_recv()
    norm_chunk(1 - p)
    relay(1)
    step(2, 3, 4)
    ts[1].wait_recv()
    norm_chunk(3 - p)
    arrived(0, 1)

    tap = [taps[pl.ds(i, 1), chan] for i in range(3)]
    pos = lax.rem(lax.broadcasted_iota(jnp.int32, (2 * half, ch), 0), LEN)

    def mix_in(c):
        x = normed[chunk(c), :]

        def proj(q):
            w = WA[:, :, q * ch:(q + 1) * ch].reshape(width, ch)
            return jnp.dot(x, w, preferred_element_type=F32)

        pr = proj(1) * proj(2)
        one = jnp.where(pos >= 1, pltpu.roll(pr, 1, 0), 0.0)
        two = jnp.where(pos >= 2, pltpu.roll(pr, 2, 0), 0.0)
        conv = tap[0] * two + tap[1] * one + tap[2] * pr
        gated[chunk(c), :] = (proj(0) * conv).astype(BF16)

    sib, zc, nb = [], [], []

    def mix_out(c):
        g = gated[chunk(c), :]
        for s in range(n_fs):
            MP[chunk(c), s * cols:(s + 1) * cols] = jnp.dot(
                g, WM[s], preferred_element_type=F32
            ).astype(BF16)
        sib.extend(start(remote(MP.at[part(c, 1 - t)], RS.at[c], sib_s.at[c], sib_r.at[c], s_dev)))

    def mix_pair(c):
        sib[c].wait_recv()
        CB[c] = (MP[part(c, t), :].astype(F32) + RS[c].astype(F32)).astype(BF16)
        zc.extend(start(remote(CB.at[c], RZ.at[c], z_s.at[c], z_r.at[c], z_dev)))

    mix_in(0)
    mix_in(1)
    arrived(2)
    mix_out(0)
    mix_out(1)
    mix_pair(0)
    mix_in(2)
    mix_out(2)
    mix_pair(1)
    mix_in(3)
    mix_out(3)
    mix_pair(2)
    mix_pair(3)

    def stream_chunk(c):
        zc[c].wait_recv()
        step_rows = 32

        def body(i, _):
            rows = pl.ds(pl.multiple_of(i * step_rows, step_rows), step_rows)
            mine = pl.ds(pl.multiple_of((2 * c + t) * half + i * step_rows, step_rows), step_rows)
            stream = tok[mine, :].astype(F32) + (CB[c, rows, :].astype(F32) + RZ[c, rows, :].astype(F32))
            n2[mine, :] = rms_scale(stream, ffn_gain[...]).astype(BF16)
            return 0

        lax.fori_loop(0, half // step_rows, body, 0)
        ref = n2.at[part(c, t)]
        nb.extend(start(remote(ref, ref, n_s.at[c], n_r.at[c], s_dev)))

    def ffn_chunks(lo, hi):
        for c in range(lo, hi):
            nb[c].wait_recv()

        def body(c, _):
            rows = chunk(c)
            x = n2[rows, :]
            for k in range(0, hid, LANES):
                n = min(LANES, hid - k)
                w = WG[:, :, 2 * k:2 * (k + n)].reshape(width, 2 * n)
                zz = jnp.dot(x, w, preferred_element_type=F32)
                g, u = zz[:, :n], zz[:, n:]
                hidden[rows, k:k + n] = (g / (1.0 + jnp.exp(-g)) * u).astype(BF16)
            return 0

        lax.fori_loop(lo, hi, body, 0)

    step(3, 5)
    step(4, 6)
    stream_chunk(0)
    step(5)
    stream_chunk(1)
    step(6, 7, 8)
    stream_chunk(2)
    arrived(3, 4, 5, 6)
    ffn_chunks(0, 3)
    stream_chunk(3)
    ffn_chunks(3, 4)

    so, qo = [], []

    def down_send(k, s):
        def body(c, _):
            both = jnp.dot(hidden[chunk(c), :], WD[s], preferred_element_type=F32).astype(BF16)
            OP[s, 0, c] = both[:half]
            OP[s, 1, c] = both[half:]
            return 0

        lax.fori_loop(0, N_CHUNKS, body, 0)
        so.extend(start(remote(OP.at[s, 1 - t], RO.at[s], o_s.at[k], o_r.at[k], s_dev)))

    def down_pair(k, s):
        so[k].wait_recv()
        for h in range(2):
            c = 2 * h + 1 - p
            ZC[s, h] = (OP[s, t, c].astype(F32) + RO[s, c].astype(F32)).astype(BF16)
        qo.extend(start(remote(ZC.at[s], RF.at[s], q_s.at[k], q_r.at[k], z_dev)))

    def finish(k, s):
        qo[k].wait_recv()
        cs = pl.ds(pl.multiple_of(s * cols, cols), cols)
        for h in range(2):
            c = 2 * h + p
            stream = tok[part(c, t), cs].astype(F32) + (CB[c, :, cs].astype(F32) + RZ[c, :, cs].astype(F32))
            branch = OP[s, t, c].astype(F32) + RO[s, c].astype(F32) + RF[s, h].astype(F32)
            out[h * half:(h + 1) * half, cs] = (stream + branch).astype(BF16)

    slots = (f, x_of, y_of, d_of)
    down_send(0, slots[0])
    step(7)
    down_pair(0, slots[0])
    step(8)
    down_send(1, slots[1])
    down_send(2, slots[2])
    down_pair(1, slots[1])
    down_pair(2, slots[2])
    arrived(7, 8)
    down_send(3, slots[3])
    finish(0, slots[0])
    down_pair(3, slots[3])
    for k in range(1, 4):
        finish(k, slots[k])
    for c in sent:
        c.wait_send()


def paired_local(
    tokens, mix_gain, w_gate_b, w_gate_c, w_conv_in, conv_taps, w_mix_out, ffn_gain,
    w_ffn_gate, w_ffn_up, w_ffn_down,
):
    chip_rows, width = tokens.shape
    n_fs = lax.axis_size("fs")
    rows_d = w_gate_b.shape[0]
    ch = w_gate_b.shape[1] // 2
    hid = w_ffn_gate.shape[1] // 2
    cols = w_mix_out.shape[1]
    half = chip_rows // 4
    group = 2 * chip_rows
    n_pieces = sum(PIECES)
    n_loads = 16 + 2 * (hid // LANES)

    def vmem(*shape):
        return pltpu.VMEM(shape, BF16)

    def dma(*shape):
        return pltpu.SemaphoreType.DMA(shape)

    return pl.pallas_call(
        layer_kernel,
        out_shape=jax.ShapeDtypeStruct((2 * half, width), BF16),
        in_specs=[pl.BlockSpec(memory_space=pl.ANY)] * 8 + [pl.BlockSpec(memory_space=pltpu.VMEM)] * 3,
        out_specs=pl.BlockSpec(memory_space=pltpu.VMEM),
        scratch_shapes=[
            vmem(group, width),
            vmem(group, width),
            vmem(group, width),
            vmem(n_fs, rows_d, 3 * ch),
            vmem(n_fs, ch, cols),
            vmem(n_fs, rows_d, 2 * hid),
            vmem(n_fs, hid, cols),
            vmem(2, rows_d, LANES),
            vmem(group, ch),
            vmem(group, width),
            vmem(N_CHUNKS, half, width),
            vmem(N_CHUNKS, half, width),
            vmem(N_CHUNKS, half, width),
            vmem(group, hid),
            vmem(n_fs, 2, N_CHUNKS, half, cols),
            vmem(n_fs, N_CHUNKS, half, cols),
            vmem(n_fs, 2, half, cols),
            vmem(n_fs, 2, half, cols),
            dma(n_loads),
            *[dma(n_pieces, 2)] * 4,
            *[dma(2)] * 4,
            *[dma(N_CHUNKS)] * 6,
            *[dma(n_fs)] * 4,
        ],
        compiler_params=pltpu.CompilerParams(
            collective_id=0, has_side_effects=True, vmem_limit_bytes=60 * 2**20
        ),
    )(
        tokens, w_gate_b, w_gate_c, w_conv_in, w_mix_out, w_ffn_gate, w_ffn_up, w_ffn_down,
        mix_gain.reshape(1, width), conv_taps, ffn_gain.reshape(1, width),
    )


def causal_mix(product_in, conv_taps):
    shaped = product_in.reshape(product_in.shape[0] // LEN, LEN, product_in.shape[1])
    padded = jnp.pad(shaped, ((0, 0), (2, 0), (0, 0)))
    convolved = (
        conv_taps[0] * padded[:, :-2]
        + conv_taps[1] * padded[:, 1:-1]
        + conv_taps[2] * padded[:, 2:]
    )
    return convolved.reshape(product_in.shape)


def general_local(
    tokens, mix_gain, w_gate_b, w_gate_c, w_conv_in, conv_taps, w_mix_out, ffn_gain,
    w_ffn_gate, w_ffn_up, w_ffn_down,
):
    def scatter(product):
        return lax.psum_scatter(
            product.astype(BF16), "tp", scatter_dimension=0, tiled=True
        ).astype(F32)

    def dot(a, b):
        return jnp.dot(a, b, preferred_element_type=F32)

    def rows(w):
        return lax.all_gather(w, "fs", axis=0, tiled=True)

    normed = rms_scale(tokens.astype(F32), mix_gain).astype(BF16)
    gate_b, gate_c, conv_in = (dot(normed, rows(w)) for w in (w_gate_b, w_gate_c, w_conv_in))
    gated = (gate_b * causal_mix(gate_c * conv_in, conv_taps)).astype(BF16)
    row_count = normed.shape[0] // lax.axis_size("tp")
    branch = scatter(dot(gated, lax.all_gather(w_mix_out, "fs", axis=1, tiled=True)))
    own = lax.dynamic_slice_in_dim(tokens, lax.axis_index("tp") * row_count, row_count, 0)
    stream = own.astype(F32) + branch
    normed_two = lax.all_gather(
        rms_scale(stream, ffn_gain).astype(BF16), "tp", axis=0, tiled=True
    )
    hidden = (jax.nn.silu(dot(normed_two, rows(w_ffn_gate))) * dot(normed_two, rows(w_ffn_up))).astype(BF16)
    ffn_branch = scatter(dot(hidden, lax.all_gather(w_ffn_down, "fs", axis=1, tiled=True)))
    return (stream + ffn_branch).astype(BF16)


def solution(mesh):
    in_specs = (
        P(("rep", "fs"), None),
        P(),
        P("fs", "tp"),
        P("fs", "tp"),
        P("fs", "tp"),
        P(None, "tp"),
        P("tp", "fs"),
        P(),
        P("fs", "tp"),
        P("fs", "tp"),
        P("tp", "fs"),
    )
    out_specs = P(("rep", "fs", "tp"), None)
    size = mesh.shape
    square = size["tp"] == 2 and size["fs"] == 4 and size["rep"] % 2 == 0

    def local(*arrays):
        rows, width = arrays[0].shape
        channels, hidden = arrays[2].shape[1], arrays[8].shape[1]
        fits = (
            square
            and rows % (4 * LEN) == 0
            and channels % (2 * LANES) == 0
            and hidden % LANES == 0
            and width % (4 * LANES) == 0
        )
        return (paired_local if fits else general_local)(*arrays)

    return jax.shard_map(local, mesh=mesh, in_specs=in_specs, out_specs=out_specs, check_vma=False)
```

time: 141 us -> 130 us (0.922)
  local copies, waits for them, and re-layouts: 8.9 us -> 2.3 us
  Pallas kernels: 132 us -> 127 us
    pallas_call x1, Pallas kernels: 132 us -> 127 us  [paired_local(): pl.pallas_call(layer_kernel, out_shape=jax.ShapeDtypeStruct((2 * half, wi...]
    slice x2 -> x0, local copies, waits for them, and re-layouts: 3.31 us -> none  [paired_local(): parts += [h[:, c:c + LANES] for h in half]]
    concatenate x1 -> x0, local copies, waits for them, and re-layouts: 3.29 us -> none  [paired_local(): wgu = jnp.concatenate(parts, axis=1)]
where the time goes in v2:
time: 130 us
  Pallas kernels  127 us (98%)
  local copies, waits for them, and re-layouts  2.3 us (2%)
    pallas_call x1, Pallas kernels, paired_local(): pl.pallas_call(layer_kernel, out_shape=jax.ShapeDtypeStruct((2 * half, wi...  127 us

profile of v2, /device:TPU:0, one launch (start us, length us, event | category | flops | bytes accessed | tf_op | source)
XLA Modules:
  0.0 129.6 jit_solution(10406739424129103501)
XLA Ops:
  0.0 127.3 %shard_map.109 = bf16[256,2048]{1,0:T(8,128)(2,1)} custom-call(bf16[512,2048]{1,0:T(8,128)(2,1)} %tokens.1, bf16[512,512]{1,0:T(8,128)(2,1)} %wb.1, bf16[512,512]{1,0:T(8,128)(2,1)} %wc.1, bf16[512,512]{1,0:T(8,128)(2,1)} %wi.1, bf16[512,512]{1,0:T(8,128)(2,1)} %wm_in.1, bf16[512,1408]{1,0:T(8,128)(2,1)} %wg_in.1, bf16[512,1408]{1,0:T(8,128)(2,1)} %wu_in.1, ...), custom_call_target="tpu_custom_call" | custom-call | tf_op jit(solution)/shard_map/pallas_call | solution.py:340
  127.3 2.3 %copy.13 = bf16[256,2048]{1,0:T(8,128)(2,1)} copy(bf16[256,2048]{1,0:T(8,128)(2,1)} %shard_map.109) | data formatting | bytes 2097152

commit v3 on v2

v3 whole, which is shorter than its diff:
```python
import jax
import jax.numpy as jnp
from jax import lax
from jax.experimental import pallas as pl
from jax.experimental.pallas import tpu as pltpu
from jax.sharding import PartitionSpec as P

LEN = 128
LANES = 128
EPSILON = 1e-06
MESH = pl.DeviceIdType.MESH
F32 = jnp.float32
BF16 = jnp.bfloat16


def rms_scale(values, gain):
    return values * lax.rsqrt(jnp.mean(values * values, axis=-1, keepdims=True) + EPSILON) * gain


N_CHUNKS = 4


def weight_pieces(rows_d, n_conv, n_mix, n_gate_up, n_down, mix_rows, down_rows):
    pieces = [(0, i * rows_d // 2, rows_d // 2, 0, n_conv) for i in range(2)]
    pieces.append((1, 0, mix_rows, 0, n_mix))
    units = n_gate_up // (2 * LANES)
    gate_up = sorted({2 * LANES * u for u in (2 * units // 5, 4 * units // 5, units)} | {0, n_gate_up})
    down = (0, n_down // 2, 3 * n_down // 4, n_down)
    for weight, rows, cuts in ((2, rows_d, gate_up), (3, down_rows, down)):
        pieces += [(weight, 0, rows, a, b - a) for a, b in zip(cuts, cuts[1:])]
    return pieces


def layer_kernel(
    tokens, wb, wc, wi, wm_in, wg_in, wu_in, wd_in, mix_gain, taps, ffn_gain,
    out,
    tok, normed, n2, WA, WM, WG, WD, tile, gated, MP, RS, BR, hidden, OP, RO, ZC, RF,
    load_sem, ds, dr, fs_, fr, tz_s, tz_r, ts_s, ts_r, g_s, g_r, sib_s, sib_r, z_s, z_r, n_s, n_r,
    o_s, o_r, q_s, q_r,
):
    n_fs, rows_d, _ = WA.shape
    ch = gated.shape[2]
    hid = hidden.shape[1]
    width = tokens.shape[1]
    half = tokens.shape[0] // 4
    cols = WD.shape[2]
    mcols = WM.shape[2]
    full, rest = hid // LANES, hid % LANES

    r = lax.axis_index("rep")
    f = lax.axis_index("fs")
    t = lax.axis_index("tp")
    p = lax.rem(r, 2)
    z_dev = {"rep": r + 1 - 2 * p}
    x_of = f + 1 - 2 * lax.rem(f, 2)
    y_of = lax.rem(f + 2, 4)
    d_of = lax.rem(x_of + 2, 4)
    x_dev, y_dev, s_dev = {"fs": x_of}, {"fs": y_of}, {"tp": 1 - t}

    def part(c, core):
        return pl.ds(pl.multiple_of((2 * c + core) * half, half), half)

    def chunk(c):
        return pl.ds(pl.multiple_of(2 * c * half, 2 * half), 2 * half)

    chan = pl.ds(pl.multiple_of(p * ch, ch), ch)
    loads = []

    def load(src, dst):
        c = pltpu.make_async_copy(src, dst, load_sem.at[len(loads)])
        c.start()
        loads.append(c)
        return c

    l_wa = []
    for k in range(2):
        rows = pl.ds(k * (rows_d // 2), rows_d // 2)
        l_wa.append([
            load(w.at[rows, chan], WA.at[f, rows, pl.ds(i * ch, ch)]) for i, w in enumerate((wb, wc, wi))
        ])
    l_tok = [
        load(tokens.at[pl.ds((2 * core + h) * half, half)], tok.at[part(2 * h + p, core)])
        for h in range(2) for core in range(2)
    ]
    barrier = pltpu.get_barrier_semaphore()
    for dev in (x_dev, y_dev, z_dev, s_dev):
        pl.semaphore_signal(barrier, inc=1, device_id=dev, device_id_type=MESH)
    pl.semaphore_wait(barrier, 4)

    def remote(src, dst, s, rcv, dev):
        return pltpu.make_async_remote_copy(
            src_ref=src, dst_ref=dst, send_sem=s, recv_sem=rcv, device_id=dev, device_id_type=MESH
        )

    bufs = (WA, WM, WG, WD)
    pieces = weight_pieces(rows_d, 3 * ch, mcols, 2 * hid, cols, WM.shape[1], hid)

    def cut(k, slot, first, parts):
        w, r0, n, c0, nc = pieces[k]
        return bufs[w].at[slot, pl.ds(r0 + first * n // 2, parts * n // 2), pl.ds(c0, nc)]

    def direct(k):
        ref = cut(k, f, 0, 2)
        return [remote(ref, ref, ds.at[k, c], dr.at[k, c], dev) for c, dev in ((0, x_dev), (1, y_dev))]

    def forward(k):
        a, b = cut(k, x_of, 0, 1), cut(k, y_of, 1, 1)
        return [
            remote(b, b, fs_.at[k, 0], fr.at[k, 0], x_dev),
            remote(a, a, fs_.at[k, 1], fr.at[k, 1], y_dev),
        ]

    sent = []

    def start(*copies):
        for c in copies:
            c.start()
            sent.append(c)
        return copies

    D, F = {}, {}

    def send(*ks):
        for k in ks:
            D[k] = start(*direct(k))

    def step(k, *more):
        for c in D[k]:
            c.wait_recv()
        F[k] = start(*forward(k))
        send(*more)

    def arrived(*ks):
        for k in ks:
            for c in F[k]:
                c.wait_recv()

    for k in range(2):
        for c in l_wa[k]:
            c.wait()
        send(k)
    for c in l_tok:
        c.wait()
    tz, ts = [], []
    for h in range(2):
        ref = tok.at[part(2 * h + p, t)]
        tz += start(remote(ref, ref, tz_s.at[h], tz_r.at[h], z_dev))

    def relay(h):
        tz[h].wait_recv()
        ref = tok.at[part(2 * h + 1 - p, t)]
        ts.extend(start(remote(ref, ref, ts_s.at[h], ts_r.at[h], s_dev)))

    def norm_chunk(c):
        def body(i, _):
            rows = pl.ds(pl.multiple_of(2 * c * half + i * 64, 64), 64)
            normed[rows, :] = rms_scale(tok[rows, :].astype(F32), mix_gain[...]).astype(BF16)
            return 0

        lax.fori_loop(0, 2 * half // 64, body, 0)

    l_rest = [load(wm_in.at[:, pl.ds(pl.multiple_of(p * mcols, mcols), mcols)], WM.at[f])]
    far = (full + (1 if rest else 0)) * LANES
    for i, w in enumerate((wg_in, wu_in)):
        for c in range(full):
            col = pl.ds(pl.multiple_of(p * far + c * LANES, LANES), LANES)
            l_rest.append(load(w.at[:, col], WG.at[f, :, pl.ds((2 * c + i) * LANES, LANES)]))
        if rest:
            l_rest.append(load(w.at[:, pl.ds(full * LANES, LANES)], tile.at[i]))
    aligned = full * LANES
    l_rest.append(load(wd_in.at[pl.ds(pl.multiple_of(p * far, LANES), aligned)], WD.at[f, pl.ds(0, aligned)]))
    if rest:
        l_rest.append(load(
            wd_in.at[pl.ds(pl.multiple_of(aligned + p * rest, rest), rest)],
            WD.at[f, pl.ds(aligned, rest)],
        ))


    norm_chunk(p)
    norm_chunk(2 + p)
    for c in l_rest:
        c.wait()
    if rest:
        gate, up = tile[0].astype(F32), tile[1].astype(F32)
        lane = lax.broadcasted_iota(jnp.int32, gate.shape, 1)
        low = jnp.where(lane < rest, gate, pltpu.roll(up, rest, 1))
        high = jnp.where(lane < rest, pltpu.roll(gate, rest, 1), up)
        WG[f, :, 2 * aligned:] = jnp.where(p == 0, low, high).astype(BF16)
    step(0, 2)
    relay(0)
    step(1)
    ts[0].wait_recv()
    norm_chunk(1 - p)
    relay(1)
    step(2, 3, 4)
    ts[1].wait_recv()
    norm_chunk(3 - p)
    arrived(0, 1)

    tap = [taps[pl.ds(i, 1), chan] for i in range(3)]
    pos = lax.rem(lax.broadcasted_iota(jnp.int32, (2 * half, ch), 0), LEN)

    def mix_in(c):
        x = normed[chunk(c), :]

        def proj(q):
            w = WA[:, :, q * ch:(q + 1) * ch].reshape(width, ch)
            return jnp.dot(x, w, preferred_element_type=F32)

        pr = proj(1) * proj(2)
        one = jnp.where(pos >= 1, pltpu.roll(pr, 1, 0), 0.0)
        two = jnp.where(pos >= 2, pltpu.roll(pr, 2, 0), 0.0)
        conv = tap[0] * two + tap[1] * one + tap[2] * pr
        gated[p, chunk(c), :] = (proj(0) * conv).astype(BF16)
        ref = gated.at[p, chunk(c)]
        gz.extend(start(remote(ref, ref, g_s.at[c], g_r.at[c], z_dev)))

    gz, sib, zc, nb = [], [], [], []

    def mix_out(c):
        gz[c].wait_recv()
        g = jnp.concatenate([gated[0, chunk(c), :], gated[1, chunk(c), :]], axis=1)
        for s in range(n_fs):
            MP[chunk(c), s * mcols:(s + 1) * mcols] = jnp.dot(
                g, WM[s], preferred_element_type=F32
            ).astype(BF16)
        sib.extend(start(remote(MP.at[part(c, 1 - t)], RS.at[c], sib_s.at[c], sib_r.at[c], s_dev)))

    def mix_pair(c):
        sib[c].wait_recv()
        BR[p, c] = (MP[part(c, t), :].astype(F32) + RS[c].astype(F32)).astype(BF16)
        zc.extend(start(remote(BR.at[p, c], BR.at[p, c], z_s.at[c], z_r.at[c], z_dev)))

    for c in range(N_CHUNKS):
        mix_in(c)
    arrived(2)
    mix_out(0)
    for c in range(1, N_CHUNKS):
        mix_out(c)
        mix_pair(c - 1)
    mix_pair(N_CHUNKS - 1)

    def stream_chunk(c):
        zc[c].wait_recv()
        step_rows = 32

        def body(i, _):
            rows = pl.ds(pl.multiple_of(i * step_rows, step_rows), step_rows)
            mine = pl.ds(pl.multiple_of((2 * c + t) * half + i * step_rows, step_rows), step_rows)
            branch = jnp.concatenate(
                [BR[q, c, rows, s * mcols:(s + 1) * mcols] for s in range(n_fs) for q in range(2)], axis=1
            )
            stream = tok[mine, :].astype(F32) + branch.astype(F32)
            n2[mine, :] = rms_scale(stream, ffn_gain[...]).astype(BF16)
            return 0

        lax.fori_loop(0, half // step_rows, body, 0)
        ref = n2.at[part(c, t)]
        nb.extend(start(remote(ref, ref, n_s.at[c], n_r.at[c], s_dev)))

    def ffn_piece(k):
        arrived(k)
        _, _, _, c0, nc = pieces[k]

        def body(i, _):
            rows = pl.ds(pl.multiple_of(4 * i * half, 4 * half), 4 * half)
            x = n2[rows, :]
            for a in range(c0, c0 + nc, 2 * LANES):
                n = min(2 * LANES, c0 + nc - a) // 2
                w = WG[:, :, a:a + 2 * n].reshape(width, 2 * n)
                zz = jnp.dot(x, w, preferred_element_type=F32)
                g, u = zz[:, :n], zz[:, n:]
                hidden[rows, a // 2:a // 2 + n] = (g / (1.0 + jnp.exp(-g)) * u).astype(BF16)
            return 0

        lax.fori_loop(0, N_CHUNKS // 2, body, 0)

    step(3, 5)
    stream_chunk(0)
    stream_chunk(1)
    step(4, 6)
    stream_chunk(2)
    stream_chunk(3)
    for c in nb:
        c.wait_recv()
    ffn_piece(3)
    step(5)
    ffn_piece(4)
    step(6, 7, 8)
    ffn_piece(5)
    ffn_piece(6)

    cuts = [pieces[k][3:] for k in (7, 8, 9)]
    blocks = [(f, 0, cols)]
    blocks += [(x_of, *cuts[0]), (y_of, *cuts[0])]
    blocks += [(x_of, *cuts[1]), (y_of, *cuts[1]), (d_of, *cuts[0])]
    blocks += [(x_of, *cuts[2]), (y_of, *cuts[2]), (d_of, *cuts[1]), (d_of, *cuts[2])]
    so, qo = [], []

    def down_send(*ks):
        for k in ks:
            s, c0, nc = blocks[k]
            cs = pl.ds(c0, nc)

            def body(i, _, s=s, c0=c0, nc=nc):
                rows = pl.ds(pl.multiple_of(4 * i * half, 4 * half), 4 * half)
                prod = jnp.dot(
                    hidden[rows, :], WD[s, :, c0:c0 + nc], preferred_element_type=F32
                ).astype(BF16)
                for e in range(4):
                    OP[s, e % 2, 2 * i + e // 2, :, c0:c0 + nc] = prod[e * half:(e + 1) * half]
                return 0

            lax.fori_loop(0, N_CHUNKS // 2, body, 0)
            so.extend(start(remote(
                OP.at[s, 1 - t, :, :, cs], RO.at[s, :, :, cs], o_s.at[k], o_r.at[k], s_dev
            )))

    def down_pair(*ks):
        for k in ks:
            so[k].wait_recv()
            s, c0, nc = blocks[k]
            cs = pl.ds(c0, nc)
            for h in range(2):
                c = 2 * h + 1 - p
                ZC[s, h, :, cs] = (OP[s, t, c, :, cs].astype(F32) + RO[s, c, :, cs].astype(F32)).astype(BF16)
            qo.extend(start(remote(
                ZC.at[s, :, :, cs], RF.at[s, :, :, cs], q_s.at[k], q_r.at[k], z_dev
            )))

    def finish(*ks):
        for k in ks:
            qo[k].wait_recv()
            s, c0, nc = blocks[k]
            for a in range(0, nc, LANES):
                lo = c0 + a
                q, at = lo // mcols, lo % mcols
                cs = pl.ds(lo, LANES)
                ms = pl.ds(pl.multiple_of(s * mcols + at, LANES), LANES)
                whole = pl.ds(pl.multiple_of(s * cols + lo, LANES), LANES)
                for h in range(2):
                    c = 2 * h + p
                    stream = tok[part(c, t), whole].astype(F32) + BR[q, c, :, ms].astype(F32)
                    branch = (
                        OP[s, t, c, :, cs].astype(F32)
                        + RO[s, c, :, cs].astype(F32)
                        + RF[s, h, :, cs].astype(F32)
                    )
                    out[h * half:(h + 1) * half, whole] = (stream + branch).astype(BF16)

    down_send(0)
    step(7, 9)
    down_pair(0)
    down_send(1, 2)
    down_pair(1, 2)
    step(8)
    down_send(3, 4)
    down_pair(3, 4)
    arrived(7)
    down_send(5)
    step(9)
    down_pair(5)
    down_send(6, 7)
    down_pair(6, 7)
    finish(0, 1, 2)
    arrived(8)
    down_send(8)
    down_pair(8)
    finish(3, 4)
    arrived(9)
    down_send(9)
    down_pair(9)
    finish(5, 6, 7, 8, 9)
    for c in sent:
        c.wait_send()


def paired_local(
    tokens, mix_gain, w_gate_b, w_gate_c, w_conv_in, conv_taps, w_mix_out, ffn_gain,
    w_ffn_gate, w_ffn_up, w_ffn_down,
):
    chip_rows, width = tokens.shape
    n_fs = lax.axis_size("fs")
    rows_d = w_gate_b.shape[0]
    ch = w_gate_b.shape[1] // 2
    hid = w_ffn_gate.shape[1] // 2
    cols = w_mix_out.shape[1]
    half = chip_rows // 4
    group = 2 * chip_rows
    n_pieces = len(weight_pieces(rows_d, 3 * ch, cols // 2, 2 * hid, cols, 2 * ch, hid))
    n_blocks = 10
    n_loads = 20 + 2 * (hid // LANES)

    def vmem(*shape):
        return pltpu.VMEM(shape, BF16)

    def dma(*shape):
        return pltpu.SemaphoreType.DMA(shape)

    return pl.pallas_call(
        layer_kernel,
        out_shape=jax.ShapeDtypeStruct((2 * half, width), BF16),
        in_specs=[pl.BlockSpec(memory_space=pl.ANY)] * 8 + [pl.BlockSpec(memory_space=pltpu.VMEM)] * 3,
        out_specs=pl.BlockSpec(memory_space=pltpu.VMEM),
        scratch_shapes=[
            vmem(group, width),
            vmem(group, width),
            vmem(group, width),
            vmem(n_fs, rows_d, 3 * ch),
            vmem(n_fs, 2 * ch, cols // 2),
            vmem(n_fs, rows_d, 2 * hid),
            vmem(n_fs, hid, cols),
            vmem(2, rows_d, LANES),
            vmem(2, group, ch),
            vmem(group, width // 2),
            vmem(N_CHUNKS, half, width // 2),
            vmem(2, N_CHUNKS, half, width // 2),
            vmem(group, hid),
            vmem(n_fs, 2, N_CHUNKS, half, cols),
            vmem(n_fs, N_CHUNKS, half, cols),
            vmem(n_fs, 2, half, cols),
            vmem(n_fs, 2, half, cols),
            dma(n_loads),
            *[dma(n_pieces, 2)] * 4,
            *[dma(2)] * 4,
            *[dma(N_CHUNKS)] * 8,
            *[dma(n_blocks)] * 4,
        ],
        compiler_params=pltpu.CompilerParams(
            collective_id=0, has_side_effects=True, vmem_limit_bytes=60 * 2**20
        ),
    )(
        tokens, w_gate_b, w_gate_c, w_conv_in, w_mix_out, w_ffn_gate, w_ffn_up, w_ffn_down,
        mix_gain.reshape(1, width), conv_taps, ffn_gain.reshape(1, width),
    )


def causal_mix(product_in, conv_taps):
    shaped = product_in.reshape(product_in.shape[0] // LEN, LEN, product_in.shape[1])
    padded = jnp.pad(shaped, ((0, 0), (2, 0), (0, 0)))
    convolved = (
        conv_taps[0] * padded[:, :-2]
        + conv_taps[1] * padded[:, 1:-1]
        + conv_taps[2] * padded[:, 2:]
    )
    return convolved.reshape(product_in.shape)


def general_local(
    tokens, mix_gain, w_gate_b, w_gate_c, w_conv_in, conv_taps, w_mix_out, ffn_gain,
    w_ffn_gate, w_ffn_up, w_ffn_down,
):
    def scatter(product):
        return lax.psum_scatter(
            product.astype(BF16), "tp", scatter_dimension=0, tiled=True
        ).astype(F32)

    def dot(a, b):
        return jnp.dot(a, b, preferred_element_type=F32)

    def rows(w):
        return lax.all_gather(w, "fs", axis=0, tiled=True)

    normed = rms_scale(tokens.astype(F32), mix_gain).astype(BF16)
    gate_b, gate_c, conv_in = (dot(normed, rows(w)) for w in (w_gate_b, w_gate_c, w_conv_in))
    gated = (gate_b * causal_mix(gate_c * conv_in, conv_taps)).astype(BF16)
    row_count = normed.shape[0] // lax.axis_size("tp")
    branch = scatter(dot(gated, lax.all_gather(w_mix_out, "fs", axis=1, tiled=True)))
    own = lax.dynamic_slice_in_dim(tokens, lax.axis_index("tp") * row_count, row_count, 0)
    stream = own.astype(F32) + branch
    normed_two = lax.all_gather(
        rms_scale(stream, ffn_gain).astype(BF16), "tp", axis=0, tiled=True
    )
    hidden = (jax.nn.silu(dot(normed_two, rows(w_ffn_gate))) * dot(normed_two, rows(w_ffn_up))).astype(BF16)
    ffn_branch = scatter(dot(hidden, lax.all_gather(w_ffn_down, "fs", axis=1, tiled=True)))
    return (stream + ffn_branch).astype(BF16)


def solution(mesh):
    in_specs = (
        P(("rep", "fs"), None),
        P(),
        P("fs", "tp"),
        P("fs", "tp"),
        P("fs", "tp"),
        P(None, "tp"),
        P("tp", "fs"),
        P(),
        P("fs", "tp"),
        P("fs", "tp"),
        P("tp", "fs"),
    )
    out_specs = P(("rep", "fs", "tp"), None)
    size = mesh.shape
    square = size["tp"] == 2 and size["fs"] == 4 and size["rep"] % 2 == 0

    def local(*arrays):
        rows, width = arrays[0].shape
        channels, hidden = arrays[2].shape[1], arrays[8].shape[1]
        fits = (
            square
            and rows % (4 * LEN) == 0
            and channels % (2 * LANES) == 0
            and hidden % LANES == 0
            and hidden >= 10 * LANES
            and width % (16 * LANES) == 0
        )
        return (paired_local if fits else general_local)(*arrays)

    return jax.shard_map(local, mesh=mesh, in_specs=in_specs, out_specs=out_specs, check_vma=False)
```

time: 130 us -> 123 us (0.946)
  Pallas kernels: 127 us -> 120 us
    pallas_call x1, Pallas kernels: 127 us -> 120 us  [paired_local(): pl.pallas_call(layer_kernel, out_shape=jax.ShapeDtypeStruct((2 * half, wi...]
where the time goes in v3:
time: 123 us
  Pallas kernels  120 us (98%)
  local copies, waits for them, and re-layouts  2.3 us (2%)
    pallas_call x1, Pallas kernels, paired_local(): pl.pallas_call(layer_kernel, out_shape=jax.ShapeDtypeStruct((2 * half, wi...  120 us

profile of v3, /device:TPU:0, one launch (start us, length us, event | category | flops | bytes accessed | tf_op | source)
XLA Modules:
  0.0 122.6 jit_solution(6747597437771759727)
XLA Ops:
  0.0 120.3 %shard_map.109 = bf16[256,2048]{1,0:T(8,128)(2,1)} custom-call(bf16[512,2048]{1,0:T(8,128)(2,1)} %tokens.1, bf16[512,512]{1,0:T(8,128)(2,1)} %wb.1, bf16[512,512]{1,0:T(8,128)(2,1)} %wc.1, bf16[512,512]{1,0:T(8,128)(2,1)} %wi.1, bf16[512,512]{1,0:T(8,128)(2,1)} %wm_in.1, bf16[512,1408]{1,0:T(8,128)(2,1)} %wg_in.1, bf16[512,1408]{1,0:T(8,128)(2,1)} %wu_in.1, ...), custom_call_target="tpu_custom_call" | custom-call | tf_op jit(solution)/shard_map/pallas_call | solution.py:400
  120.3 2.3 %copy.13 = bf16[256,2048]{1,0:T(8,128)(2,1)} copy(bf16[256,2048]{1,0:T(8,128)(2,1)} %shard_map.109) | data formatting | bytes 2097152

commit v4 on v3

--- a/solution.py
+++ b/solution.py
@@ -32,9 +32,9 @@
 
 
 def layer_kernel(
-    tokens, wb, wc, wi, wm_in, wg_in, wu_in, wd_in, mix_gain, taps, ffn_gain,
+    tokens, wb, wc, wi, wm_in, wg_in, wu_in, wd_in, mix_gain_in, taps_in, ffn_gain_in,
     out,
-    tok, normed, n2, WA, WM, WG, WD, tile, gated, MP, RS, BR, hidden, OP, RO, ZC, RF,
+    tok, normed, n2, WA, WM, WG, WD, tile, gated, MP, RS, BR, hidden, OP, RO, ZC, RF, mix_gain, taps, ffn_gain,
     load_sem, ds, dr, fs_, fr, tz_s, tz_r, ts_s, ts_r, g_s, g_r, sib_s, sib_r, z_s, z_r, n_s, n_r,
     o_s, o_r, q_s, q_r,
 ):
@@ -63,6 +63,10 @@
     def chunk(c):
         return pl.ds(pl.multiple_of(2 * c * half, 2 * half), 2 * half)
 
+    barrier = pltpu.get_barrier_semaphore()
+    for dev in (x_dev, y_dev, z_dev, s_dev):
+        pl.semaphore_signal(barrier, inc=1, device_id=dev, device_id_type=MESH)
+
     chan = pl.ds(pl.multiple_of(p * ch, ch), ch)
     loads = []
 
@@ -82,9 +86,9 @@
         load(tokens.at[pl.ds((2 * core + h) * half, half)], tok.at[part(2 * h + p, core)])
         for h in range(2) for core in range(2)
     ]
-    barrier = pltpu.get_barrier_semaphore()
-    for dev in (x_dev, y_dev, z_dev, s_dev):
-        pl.semaphore_signal(barrier, inc=1, device_id=dev, device_id_type=MESH)
+    l_small = [
+        load(a, b) for a, b in ((mix_gain_in, mix_gain), (taps_in, taps), (ffn_gain_in, ffn_gain))
+    ]
     pl.semaphore_wait(barrier, 4)
 
     def remote(src, dst, s, rcv, dev):
@@ -139,7 +143,7 @@
         for c in l_wa[k]:
             c.wait()
         send(k)
-    for c in l_tok:
+    for c in l_tok + l_small:
         c.wait()
     tz, ts = [], []
     for h in range(2):
@@ -400,7 +404,7 @@
     return pl.pallas_call(
         layer_kernel,
         out_shape=jax.ShapeDtypeStruct((2 * half, width), BF16),
-        in_specs=[pl.BlockSpec(memory_space=pl.ANY)] * 8 + [pl.BlockSpec(memory_space=pltpu.VMEM)] * 3,
+        in_specs=[pl.BlockSpec(memory_space=pl.ANY)] * 11,
         out_specs=pl.BlockSpec(memory_space=pltpu.VMEM),
         scratch_shapes=[
             vmem(group, width),
@@ -420,6 +424,9 @@
             vmem(n_fs, N_CHUNKS, half, cols),
             vmem(n_fs, 2, half, cols),
             vmem(n_fs, 2, half, cols),
+            pltpu.VMEM((1, width), F32),
+            pltpu.VMEM(conv_taps.shape, F32),
+            pltpu.VMEM((1, width), F32),
             dma(n_loads),
             *[dma(n_pieces, 2)] * 4,
             *[dma(2)] * 4,

time: 123 us -> 122 us (level)
  no operation moved by 1% of the time
where the time goes in v4:
time: 122 us
  Pallas kernels  120 us (98%)
  local copies, waits for them, and re-layouts  2.3 us (2%)
    pallas_call x1, Pallas kernels, paired_local(): pl.pallas_call(layer_kernel, out_shape=jax.ShapeDtypeStruct((2 * half, wi...  120 us

profile of v4, /device:TPU:0, one launch (start us, length us, event | category | flops | bytes accessed | tf_op | source)
XLA Modules:
  0.0 121.8 jit_solution(2258785276280302968)
XLA Ops:
  0.0 119.5 %shard_map.109 = bf16[256,2048]{1,0:T(8,128)(2,1)} custom-call(bf16[512,2048]{1,0:T(8,128)(2,1)} %tokens.1, bf16[512,512]{1,0:T(8,128)(2,1)} %wb.1, bf16[512,512]{1,0:T(8,128)(2,1)} %wc.1, bf16[512,512]{1,0:T(8,128)(2,1)} %wi.1, bf16[512,512]{1,0:T(8,128)(2,1)} %wm_in.1, bf16[512,1408]{1,0:T(8,128)(2,1)} %wg_in.1, bf16[512,1408]{1,0:T(8,128)(2,1)} %wu_in.1, ...), custom_call_target="tpu_custom_call" | custom-call | tf_op jit(solution)/shard_map/pallas_call | solution.py:404
  119.5 2.3 %copy.13 = bf16[256,2048]{1,0:T(8,128)(2,1)} copy(bf16[256,2048]{1,0:T(8,128)(2,1)} %shard_map.109) | data formatting | bytes 2097152
